TPU v7x, 32 devices: a whole 2x2x4 slice. The times are simulated.
32 devices in a mesh: grp: 2 (over y), kv: 4 (over z), tp: 4 (over x, core).
Axes of the slice: x: 2, y: 2, z: 4, core: 2. Of those that a mesh axis runs over, the one named last changes fastest.
Arguments:
- stream_in: bfloat16 [96, 4096], P(('grp', 'tp'), 'kv'), parts along dimension 0, may hold values from -40 to 40
- positions: int32 [96], P(('grp', 'kv')), parts along dimension 0, may hold values from 1024 to 32767
- ret_state: float32 [96, 16, 128, 128], P(('grp', 'kv'), 'tp'), parts along dimension 0, may hold values from -0.6 to 0.6
- first_gain: float32 [4096], P('kv'), may hold values from 0.1 to 1.9
- first_gate: bfloat16 [4096, 11008], P('kv', 'tp'), may hold values from -0.09375 to 0.09375
- first_up: bfloat16 [4096, 11008], P('kv', 'tp'), may hold values from -0.09375 to 0.09375
- first_down: bfloat16 [11008, 4096], P('tp', 'kv'), may hold values from -0.1875 to 0.1875
- mix_gain: float32 [4096], P('kv'), may hold values from 0.1 to 1.9
- w_query: bfloat16 [4096, 2048], P('kv', 'tp'), may hold values from -0.09375 to 0.09375
- w_key: bfloat16 [4096, 2048], P('kv', 'tp'), may hold values from -0.09375 to 0.09375
- w_value: bfloat16 [4096, 2048], P('kv', 'tp'), may hold values from -0.09375 to 0.09375
- w_outgate: bfloat16 [4096, 2048], P('kv', 'tp'), may hold values from -0.09375 to 0.09375
- w_out: bfloat16 [2048, 4096], P('tp', 'kv'), may hold values from -0.21875 to 0.21875
- head_gain: float32 [2048], P('tp'), may hold values from 0.1 to 1.9
- second_gain: float32 [4096], P('kv'), may hold values from 0.1 to 1.9
- second_gate: bfloat16 [4096, 11008], P('kv', 'tp'), may hold values from -0.09375 to 0.09375
- second_up: bfloat16 [4096, 11008], P('kv', 'tp'), may hold values from -0.09375 to 0.09375
- second_down: bfloat16 [11008, 4096], P('tp', 'kv'), may hold values from -0.1875 to 0.1875
Outputs:
- stream_out: bfloat16 [96, 4096], P(('grp', 'tp'), 'kv'), parts along dimension 0
- new_state: float32 [96, 16, 128, 128], P(('grp', 'kv'), 'tp'), parts along dimension 0
There are 2 independent parts, one for each index of `grp`. A program takes and returns all parts, laid end to end along the dimension named above; an argument that names none is the same for every part. Nothing has to cross between parts.
All inputs are finite; a program needn't handle non-finite values.
Results may differ from a plain program's by a relative error of at most 0.03.
Values may be sent and summed in bfloat16 or wider, within the bound.
A program may use at most 128 MiB of HBM per device.

v0:
```python
import jax
import jax.numpy as jnp
from jax import lax
from jax.sharding import PartitionSpec as P

D = 4096
EPS_NORM = 1e-06
EPS_GROUP = 1e-05


def widen_rows(stream_rows):
    return lax.all_gather(stream_rows, "tp", axis=0, tiled=True)


def prepare(stream, norm_gain):
    widened = stream.astype(jnp.float32)
    squares = jnp.sum(widened * widened, axis=1)
    scaled = (widened * norm_gain).astype(jnp.bfloat16)
    return (squares, scaled)


def feed_forward(stream, norm_gain, w_gate, w_up):
    squares, scaled = prepare(stream, norm_gain)
    gate_part = jnp.dot(scaled, w_gate, preferred_element_type=jnp.float32)
    up_part = jnp.dot(scaled, w_up, preferred_element_type=jnp.float32)
    gate_part, up_part, squares = (
        lax.psum(gate_part.astype(jnp.bfloat16), "kv").astype(jnp.float32),
        lax.psum(up_part.astype(jnp.bfloat16), "kv").astype(jnp.float32),
        lax.psum(squares.astype(jnp.bfloat16), "kv").astype(jnp.float32),
    )
    factor = lax.rsqrt(squares / D + EPS_NORM)[:, None]
    return (jax.nn.silu(factor * gate_part) * (factor * up_part)).astype(jnp.bfloat16)


def advance(stream, inputs_back, weight_back, factor_branch):
    row_count = stream.shape[0] // lax.axis_size("tp")
    row_share = lax.psum_scatter(
        jnp.dot(inputs_back, weight_back, preferred_element_type=jnp.float32).astype(jnp.bfloat16),
        "tp",
        scatter_dimension=0,
        tiled=True,
    ).astype(jnp.float32)
    own_rows = lax.dynamic_slice_in_dim(stream, lax.axis_index("tp") * row_count, row_count, 0)
    return (own_rows.astype(jnp.float32) + factor_branch * row_share).astype(jnp.bfloat16)


def rotate(values_in, cosine, sine_part):
    half_dim = values_in.shape[-1] // 2
    lower_half = values_in[..., :half_dim]
    upper_half = values_in[..., half_dim:]
    return jnp.concatenate(
        [
            lower_half * cosine - upper_half * sine_part,
            lower_half * sine_part + upper_half * cosine,
        ],
        axis=-1,
    )


def retention(
    stream, norm_gain, w_query, w_key, w_value, w_outgate, head_gain, state_old, positions
):
    squares, scaled = prepare(stream, norm_gain)
    query_part = jnp.dot(scaled, w_query, preferred_element_type=jnp.float32)
    key_part = jnp.dot(scaled, w_key, preferred_element_type=jnp.float32)
    value_part = jnp.dot(scaled, w_value, preferred_element_type=jnp.float32)
    gate_part = jnp.dot(scaled, w_outgate, preferred_element_type=jnp.float32)
    query_part, key_part, value_part, gate_part, squares = (
        lax.psum_scatter(
            query_part.astype(jnp.bfloat16), "kv", scatter_dimension=0, tiled=True
        ).astype(jnp.float32),
        lax.psum_scatter(
            key_part.astype(jnp.bfloat16), "kv", scatter_dimension=0, tiled=True
        ).astype(jnp.float32),
        lax.psum_scatter(
            value_part.astype(jnp.bfloat16), "kv", scatter_dimension=0, tiled=True
        ).astype(jnp.float32),
        lax.psum_scatter(
            gate_part.astype(jnp.bfloat16), "kv", scatter_dimension=0, tiled=True
        ).astype(jnp.float32),
        lax.psum_scatter(
            squares.astype(jnp.bfloat16), "kv", scatter_dimension=0, tiled=True
        ).astype(jnp.float32),
    )
    factor = lax.rsqrt(squares / D + EPS_NORM)[:, None]
    sequences = state_old.shape[0]
    head_count = state_old.shape[1]
    width_head = state_old.shape[2]
    shape_heads = (sequences, head_count, width_head)
    queries = (factor * query_part).reshape(shape_heads)
    key_vec = (factor * key_part).reshape(shape_heads)
    values_new = (factor * value_part).reshape(shape_heads)
    gate_pre = (factor * gate_part).reshape(shape_heads)
    half_dim = width_head // 2
    inverse = 10000.0 ** (-jnp.arange(half_dim, dtype=jnp.float32) / half_dim)
    angles = positions.astype(jnp.float32)[:, None] * inverse[None, :]
    cosine = jnp.cos(angles)[:, None, :]
    sine_part = jnp.sin(angles)[:, None, :]
    queries = rotate(queries, cosine, sine_part)
    key_vec = rotate(key_vec, cosine, sine_part) * width_head ** (-0.5)
    head_ids = (lax.axis_index("tp") * head_count + jnp.arange(head_count)).astype(jnp.float32)
    decays = jnp.exp(jnp.log1p(-(2.0 ** (-5.0 - head_ids))))
    carried = jnp.einsum("shd,shde->she", queries, state_old, precision=lax.Precision.HIGHEST)
    within = jnp.sum(queries * key_vec, axis=-1, keepdims=True)
    mixture = decays[None, :, None] * carried + within * values_new
    new_state = (
        decays[None, :, None, None] * state_old + key_vec[..., :, None] * values_new[..., None, :]
    )
    average = jnp.mean(mixture, axis=-1, keepdims=True)
    centered = mixture - average
    variance = jnp.mean(centered * centered, axis=-1, keepdims=True)
    normed = centered * lax.rsqrt(variance + EPS_GROUP) * head_gain.reshape(head_count, width_head)
    ret_out = (
        (jax.nn.silu(gate_pre) * normed)
        .astype(jnp.bfloat16)
        .reshape(sequences, head_count * width_head)
    )
    return (lax.all_gather(ret_out, "kv", axis=0, tiled=True), new_state)


def per_device(
    stream_in,
    positions,
    ret_state,
    first_gain,
    first_gate,
    first_up,
    first_down,
    mix_gain,
    w_query,
    w_key,
    w_value,
    w_outgate,
    w_out,
    head_gain,
    second_gain,
    second_gate,
    second_up,
    second_down,
):
    stream = widen_rows(stream_in)
    hidden = feed_forward(stream, first_gain, first_gate, first_up)
    stream = advance(stream, hidden, first_down, 0.5)
    stream = widen_rows(stream)
    ret_out, new_state = retention(
        stream, mix_gain, w_query, w_key, w_value, w_outgate, head_gain, ret_state, positions
    )
    stream = advance(stream, ret_out, w_out, 1.0)
    stream = widen_rows(stream)
    hidden = feed_forward(stream, second_gain, second_gate, second_up)
    stream = advance(stream, hidden, second_down, 0.5)
    return (stream, new_state)


def solution(mesh):
    in_specs = (
        P(("grp", "tp"), "kv"),
        P(("grp", "kv")),
        P(("grp", "kv"), "tp", None, None),
        P("kv"),
        P("kv", "tp"),
        P("kv", "tp"),
        P("tp", "kv"),
        P("kv"),
        P("kv", "tp"),
        P("kv", "tp"),
        P("kv", "tp"),
        P("kv", "tp"),
        P("tp", "kv"),
        P("tp"),
        P("kv"),
        P("kv", "tp"),
        P("kv", "tp"),
        P("tp", "kv"),
    )
    out_specs = (P(("grp", "tp"), "kv"), P(("grp", "kv"), "tp", None, None))
    return jax.shard_map(
        per_device, mesh=mesh, in_specs=in_specs, out_specs=out_specs, check_vma=False
    )
```

profile of v0, /device:TPU:1, one launch (start us, length us, event | category | flops | bytes accessed | tf_op | source)
XLA Modules:
  0.0 235.9 jit_solution(9021519236069175945)
XLA Ops:
  7.2 6.7 %all-gather = bf16[4,12,1024]{2,1,0:T(8,128)(2,1)S(1)} all-gather(bf16[1,12,1024]{2,1,0:T(8,128)(2,1)} %bitcast.43), channel_id=1, replica_groups=mesh['grp'=2,'kv'=4,'tp'=4] {'tp'}, dimensions={0}, use_global_device_ids=true | all-gather | bytes 122880 | tf_op jit(solution)/shard_map/all_gather | solution.py:12
  14.0 5.3 %convolution_convert_fusion.2 = bf16[48,2752]{1,0:T(8,128)(2,1)} fusion(bf16[1024,2752]{0,1:T(8,128)(2,1)} %param.23, bf16[48,1024]{1,0:T(8,128)(2,1)S(1)} %reshape.132, f32[1024]{0:T(1024)} %param.21), kind=kOutput, calls=%fused_computation.3 | convolution fusion | flops 270812160 | bytes 6002688 | tf_op jit(solution)/shard_map/dot_general | solution.py:25
  19.3 2.5 %convolution_convert_fusion.3 = bf16[48,2752]{1,0:T(8,128)(2,1)} fusion(bf16[1024,2752]{0,1:T(8,128)(2,1)S(1)} %copy-done.1, bf16[48,1024]{1,0:T(8,128)(2,1)S(1)} %reshape.132, f32[1024]{0:T(1024)S(1)} %copy-done.5), kind=kOutput, calls=%fused_computation.4 | convolution fusion | flops 270812160 | bytes 6002688 | tf_op jit(solution)/shard_map/dot_general | solution.py:24
  21.9 0.1 fusion.14
  22.0 10.6 %psum.42 = bf16[48]{0:T(256)(128)(2,1)S(1)} all-reduce(bf16[48]{0:T(256)(128)(2,1)S(1)} %fusion.14), channel_id=1, replica_groups=mesh['grp'=2,'kv'=4,'tp'=4] {'kv'}, use_global_device_ids=true, to_apply=%region_1.0 | all-reduce | flops 48 | bytes 192 | tf_op jit(solution)/shard_map/psum | solution.py:29
  32.7 28.6 %all-reduce.23.cloned.1.call-done = (bf16[48,2752]{1,0:T(8,128)(2,1)}, bf16[48,2752]{1,0:T(8,128)(2,1)}) async-done(((bf16[48,2752]{1,0:T(8,128)(2,1)}, bf16[48,2752]{1,0:T(8,128)(2,1)}), (bf16[48,2752]{1,0:T(8,128)(2,1)}, bf16[48,2752]{1,0:T(8,128)(2,1)})) %all-reduce.23.cloned.1.call-update) | async-done | bytes 528400 | tf_op jit(solution)/shard_map/psum | solution.py:28
  61.3 3.9 %convolution_convert_fusion.6 = bf16[48,1024]{1,0:T(8,128)(2,1)S(1)} fusion(bf16[2752,1024]{1,0:T(8,128)(2,1)} %param.24, bf16[48,2752]{1,0:T(8,128)(2,1)} %get-tuple-element.4, bf16[48,2752]{1,0:T(8,128)(2,1)} %get-tuple-element.5, f32[48]{0:T(128)S(1)} %add_rsqrt_fusion.2), kind=kOutput, calls=%fused_computation.8 | convolution fusion | flops 271902720 | bytes 6262976 | tf_op jit(solution)/shard_map/dot_general | solution.py:38
  65.3 7.6 %fusion = bf16[16,1024]{1,0:T(8,128)(2,1)S(1)} fusion(bf16[48,1024]{1,0:T(8,128)(2,1)S(1)} %convolution_convert_fusion.6), kind=kCustom, calls=%all-reduce-scatter | all-reduce-scatter fusion | flops 65537 | bytes 131584
  72.9 4.2 %collective-permute-start = (bf16[12,1024]{1,0:T(8,128)(2,1)S(1)}, bf16[12,1024]{1,0:T(8,128)(2,1)S(1)}, u32[]{:S(2)}, u32[]{:S(2)}) collective-permute-start(bf16[12,1024]{1,0:T(8,128)(2,1)S(1)} %slice.20), channel_id=1, source_target_pairs={{0,1},{1,2},{2,3},{4,5},{5,6},{6,7},{8,9},{9,10},{10,11},{12,13},{... | collective-permute-start | bytes 73736
  77.1 0.6 dynamic-slice.18
  78.4 0.6 fusion.39
  80.3 0.2 concatenate.12
  80.5 4.3 %all-gather.1 = bf16[4,12,1024]{2,1,0:T(8,128)(2,1)S(1)} all-gather(bf16[1,12,1024]{2,1,0:T(8,128)(2,1)S(1)} %fusion.28), channel_id=1, replica_groups=mesh['grp'=2,'kv'=4,'tp'=4] {'tp'}, dimensions={0}, use_global_device_ids=true | all-gather | bytes 122880 | tf_op jit(solution)/shard_map/all_gather | solution.py:12
  84.9 8.9 %all-reduce.1 = bf16[48]{0:T(256)(128)(2,1)S(1)} all-reduce(bf16[48]{0:T(256)(128)(2,1)S(1)} %fusion.16), channel_id=3, replica_groups=mesh['grp'=2,'kv'=4,'tp'=4] {'kv'}, use_global_device_ids=true, to_apply=%region_6.7.clone | all-reduce | flops 48 | bytes 192
  93.8 0.3 convolution_convert_fusion.9
  94.1 0.3 convolution_convert_fusion.8
  94.4 1.5 convolution_convert_fusion.7
  95.9 1.5 convolution_convert_fusion.10
  97.4 10.5 %fusion.38 = (bf16[16,512]{1,0:T(8,128)(2,1)S(1)}, bf16[16,512]{1,0:T(8,128)(2,1)S(1)}, bf16[16,512]{1,0:T(8,128)(2,1)S(1)}, bf16[16,512]{1,0:T(8,128)(2,1)S(1)}) fusion(bf16[48,512]{1,0:T(8,128)(2,1)S(1)} %convolution_convert_fusion.10, bf16[48,512]{1,0:T(8,128)(2,1)S(1)} %convolution_convert_fusion.7, bf16[48,512]{1,0:T(8,128)(2,1)S(1)} %convolution_convert_fusion.9, ...), kind=kCustom, calls=%all-reduce-scatter.7 | all-reduce-scatter fusion | flops 131073 | bytes 262656
  108.0 1.6 collective-permute-start.3
  109.6 1.9 collective-permute-start.2
  111.5 3.3 %collective-permute-start.4 = (bf16[12,512]{1,0:T(8,128)(2,1)S(1)}, bf16[12,512]{1,0:T(8,128)(2,1)S(1)}, u32[]{:S(2)}, u32[]{:S(2)}) collective-permute-start(bf16[12,512]{1,0:T(8,128)(2,1)S(1)} %slice.24), channel_id=1, source_target_pairs={{0,4},{4,8},{8,12},{1,5},{5,9},{9,13},{2,6},{6,10},{10,14},{3,7},{... | collective-permute-start | bytes 36872
  114.8 1.9 collective-permute-start.1
  116.9 0.1 concatenate.15
  117.0 0.2 concatenate.14
  117.2 0.2 concatenate.16
  117.4 0.3 collective-permute-done.1
  118.1 4.6 %fusion.41 = f32[12,4,1,128]{3,2,1,0:T(1,128)S(1)} fusion(f32[12,4,128,1]{2,3,1,0:T(1,128)S(1)} %bitcast.42, f32[12,4,128,128]{3,2,1,0:T(8,128)} %param.20), kind=kOutput, calls=%fused_computation.70 | convolution fusion | flops 9437184 | bytes 3194880 | tf_op jit(solution)/shard_map/shd,shde->she/dot_general | solution.py:103
  122.7 0.2 fusion.40
  122.9 0.2 multiply_reduce_fusion
  123.2 10.3 %all-gather.2 = bf16[4,12,512]{2,1,0:T(8,128)(2,1)S(1)} all-gather(bf16[1,12,512]{2,1,0:T(8,128)(2,1)S(1)} %reshape.135), channel_id=1, replica_groups=mesh['grp'=2,'kv'=4,'tp'=4] {'kv'}, dimensions={0}, use_global_device_ids=true | all-gather | bytes 61440 | tf_op jit(solution)/shard_map/all_gather | solution.py:118
  133.5 0.3 convolution_convert_fusion.5
  133.8 15.0 %fusion.5 = bf16[16,1024]{1,0:T(8,128)(2,1)S(1)} fusion(bf16[48,1024]{1,0:T(8,128)(2,1)S(1)} %convolution_convert_fusion.5), kind=kCustom, calls=%all-reduce-scatter.5 | all-reduce-scatter fusion | flops 65537 | bytes 131584
  148.8 4.2 %collective-permute-start.5 = (bf16[12,1024]{1,0:T(8,128)(2,1)S(1)}, bf16[12,1024]{1,0:T(8,128)(2,1)S(1)}, u32[]{:S(2)}, u32[]{:S(2)}) collective-permute-start(bf16[12,1024]{1,0:T(8,128)(2,1)S(1)} %slice.25), channel_id=1, source_target_pairs={{0,1},{1,2},{2,3},{4,5},{5,6},{6,7},{8,9},{9,10},{10,11},{12,13},{... | collective-permute-start | bytes 73736
  153.1 1.0 collective-permute-done.5
  154.1 0.1 concatenate.17
  154.2 6.3 %all-gather.3 = bf16[4,12,1024]{2,1,0:T(8,128)(2,1)S(1)} all-gather(bf16[1,12,1024]{2,1,0:T(8,128)(2,1)S(1)} %fusion.29), channel_id=1, replica_groups=mesh['grp'=2,'kv'=4,'tp'=4] {'tp'}, dimensions={0}, use_global_device_ids=true | all-gather | bytes 122880 | tf_op jit(solution)/shard_map/all_gather | solution.py:12
  160.6 5.1 %convolution_convert_fusion = bf16[48,2752]{1,0:T(8,128)(2,1)} fusion(bf16[1024,2752]{0,1:T(8,128)(2,1)} %param.34, bf16[48,1024]{1,0:T(8,128)(2,1)S(1)} %reshape.138, f32[1024]{0:T(1024)S(1)} %copy-done.6), kind=kOutput, calls=%fused_computation.1 | convolution fusion | flops 270812160 | bytes 6002688 | tf_op jit(solution)/shard_map/dot_general | solution.py:25
  165.7 5.1 %convolution_convert_fusion.1 = bf16[48,2752]{1,0:T(8,128)(2,1)} fusion(bf16[1024,2752]{0,1:T(8,128)(2,1)} %param.33, bf16[48,1024]{1,0:T(8,128)(2,1)S(1)} %reshape.138, f32[1024]{0:T(1024)S(1)} %copy-done.6), kind=kOutput, calls=%fused_computation.2 | convolution fusion | flops 270812160 | bytes 6002688 | tf_op jit(solution)/shard_map/dot_general | solution.py:24
  170.8 0.1 fusion.18
  170.9 8.8 %psum.45 = bf16[48]{0:T(256)(128)(2,1)S(1)} all-reduce(bf16[48]{0:T(256)(128)(2,1)S(1)} %fusion.18), channel_id=1, replica_groups=mesh['grp'=2,'kv'=4,'tp'=4] {'kv'}, use_global_device_ids=true, to_apply=%region_16.17 | all-reduce | flops 48 | bytes 192 | tf_op jit(solution)/shard_map/psum | solution.py:29
  179.8 29.1 %all-reduce.21.cloned.1.call-done = (bf16[48,2752]{1,0:T(8,128)(2,1)}, bf16[48,2752]{1,0:T(8,128)(2,1)}) async-done(((bf16[48,2752]{1,0:T(8,128)(2,1)}, bf16[48,2752]{1,0:T(8,128)(2,1)}), (bf16[48,2752]{1,0:T(8,128)(2,1)}, bf16[48,2752]{1,0:T(8,128)(2,1)})) %all-reduce.21.cloned.1.call-update) | async-done | bytes 528400 | tf_op jit(solution)/shard_map/psum | solution.py:28
  208.9 3.9 %convolution_convert_fusion.4 = bf16[48,1024]{1,0:T(8,128)(2,1)S(1)} fusion(bf16[2752,1024]{1,0:T(8,128)(2,1)} %param.35, bf16[48,2752]{1,0:T(8,128)(2,1)} %get-tuple-element.2, bf16[48,2752]{1,0:T(8,128)(2,1)} %get-tuple-element.3, f32[48]{0:T(128)S(1)} %add_rsqrt_fusion.1), kind=kOutput, calls=%fused_computation.6 | convolution fusion | flops 271902720 | bytes 6262976 | tf_op jit(solution)/shard_map/dot_general | solution.py:38
  212.9 7.6 %fusion.6 = bf16[16,1024]{1,0:T(8,128)(2,1)S(1)} fusion(bf16[48,1024]{1,0:T(8,128)(2,1)S(1)} %convolution_convert_fusion.4), kind=kCustom, calls=%all-reduce-scatter.6 | all-reduce-scatter fusion | flops 65537 | bytes 131584
  220.5 4.2 %collective-permute-start.6 = (bf16[12,1024]{1,0:T(8,128)(2,1)S(1)}, bf16[12,1024]{1,0:T(8,128)(2,1)S(1)}, u32[]{:S(2)}, u32[]{:S(2)}) collective-permute-start(bf16[12,1024]{1,0:T(8,128)(2,1)S(1)} %slice.26), channel_id=1, source_target_pairs={{0,1},{1,2},{2,3},{4,5},{5,6},{6,7},{8,9},{9,10},{10,11},{12,13},{... | collective-permute-start | bytes 73736
  224.7 3.6 %multiply_add_fusion = f32[12,4,128,128]{3,2,1,0:T(8,128)} fusion(f32[12,4,128,128]{3,2,1,0:T(8,128)} %param.20, f32[12,4,128]{2,1,0:T(4,128)S(1)} %reshape.129, f32[12,4,128]{2,1,0:T(4,128)S(1)} %get-tuple-element.31, f32[4]{0:T(128)S(1)} %log-plus-one_exponential_fusion), kind=kLoop, calls=%fused_computation.5 | loop fusion | flops 2359296 | bytes 6340624 | tf_op jit(solution)/shard_map/add | solution.py:107
  228.3 0.2 concatenate.18
  228.4 0.7 add_convert_fusion
  (64 shorter events, 1.3 us)
Async XLA Ops:
  7.2 126.4 %copy-start = (bf16[512,1024]{1,0:T(8,128)(2,1)S(1)}, bf16[512,1024]{1,0:T(8,128)(2,1)}, u32[]{:S(2)}) copy-start(bf16[512,1024]{1,0:T(8,128)(2,1)} %param.30) | copy-start | bytes 3145732
  7.2 12.1 %copy-start.5 = (f32[1024]{0:T(1024)S(1)}, f32[1024]{0:T(1024)}, u32[]{:S(2)}) copy-start(f32[1024]{0:T(1024)} %param.21) | copy-start | bytes 12292
  7.2 54.1 %all-reduce.23.cloned.1.call-start = ((), (), s32[]{:S(2)}) async-start(), calls=%async_computation.1 | async-start | bytes 1081344 | tf_op jit(solution)/shard_map/psum | solution.py:28
  14.0 5.3 %copy-start.1 = (bf16[1024,2752]{0,1:T(8,128)(2,1)S(1)}, bf16[1024,2752]{0,1:T(8,128)(2,1)}, u32[]{:S(2)}) copy-start(bf16[1024,2752]{0,1:T(8,128)(2,1)} %param.22) | copy-start | bytes 16908292
  14.0 8.0 %copy-start.10 = (s32[12]{0:T(128)S(1)}, s32[12]{0:T(128)}, u32[]{:S(2)}) copy-start(s32[12]{0:T(128)} %param.19) | copy-start | bytes 148
  19.3 57.9 %copy-start.9 = (u32[32]{0:T(128)S(1)}, u32[32]{0:T(128)}, u32[]{:S(2)}) copy-start(u32[32]{0:T(128)} %constant.53) | copy-start | bytes 388
  19.3 59.1 %copy-start.8 = (u32[32]{0:T(128)S(1)}, u32[32]{0:T(128)}, u32[]{:S(2)}) copy-start(u32[32]{0:T(128)} %constant.57) | copy-start | bytes 388
  21.8 72.0 %copy-start.2 = (bf16[1024,512]{1,0:T(8,128)(2,1)S(1)}, bf16[1024,512]{1,0:T(8,128)(2,1)}, u32[]{:S(2)}) copy-start(bf16[1024,512]{1,0:T(8,128)(2,1)} %param.26) | copy-start | bytes 3145732
  21.8 72.0 %copy-start.4 = (f32[1024]{0:T(1024)S(1)}, f32[1024]{0:T(1024)}, u32[]{:S(2)}) copy-start(f32[1024]{0:T(1024)} %param.25) | copy-start | bytes 12292
  21.8 72.3 %copy-start.3 = (bf16[1024,512]{1,0:T(8,128)(2,1)S(1)}, bf16[1024,512]{1,0:T(8,128)(2,1)}, u32[]{:S(2)}) copy-start(bf16[1024,512]{1,0:T(8,128)(2,1)} %param.27) | copy-start | bytes 3145732
  21.8 187.1 %all-reduce.21.cloned.1.call-start = ((), (), s32[]{:S(2)}) async-start(), calls=%async_computation | async-start | bytes 1081344 | tf_op jit(solution)/shard_map/psum | solution.py:28
  65.3 57.8 %copy-start.7 = (f32[512]{0:T(512)S(1)}, f32[512]{0:T(512)}, u32[]{:S(2)}) copy-start(f32[512]{0:T(512)} %param.31) | copy-start | bytes 6148
  72.9 7.4 %collective-permute-start = (bf16[12,1024]{1,0:T(8,128)(2,1)S(1)}, bf16[12,1024]{1,0:T(8,128)(2,1)S(1)}, u32[]{:S(2)}, u32[]{:S(2)}) collective-permute-start(bf16[12,1024]{1,0:T(8,128)(2,1)S(1)} %slice.20), channel_id=1, source_target_pairs={{0,1},{1,2},{2,3},{4,5},{5,6},{6,7},{8,9},{9,10},{10,11},{12,13},{... | collective-permute-start | bytes 73736
  94.1 66.5 %copy-start.6 = (f32[1024]{0:T(1024)S(1)}, f32[1024]{0:T(1024)}, u32[]{:S(2)}) copy-start(f32[1024]{0:T(1024)} %param.32) | copy-start | bytes 12292
  108.0 8.9 %collective-permute-start.3 = (bf16[12,512]{1,0:T(8,128)(2,1)S(1)}, bf16[12,512]{1,0:T(8,128)(2,1)S(1)}, u32[]{:S(2)}, u32[]{:S(2)}) collective-permute-start(bf16[12,512]{1,0:T(8,128)(2,1)S(1)} %slice.23), channel_id=1, source_target_pairs={{0,4},{4,8},{8,12},{1,5},{5,9},{9,13},{2,6},{6,10},{10,14},{3,7},{... | collective-permute-start | bytes 36872
  109.6 7.4 %collective-permute-start.2 = (bf16[12,512]{1,0:T(8,128)(2,1)S(1)}, bf16[12,512]{1,0:T(8,128)(2,1)S(1)}, u32[]{:S(2)}, u32[]{:S(2)}) collective-permute-start(bf16[12,512]{1,0:T(8,128)(2,1)S(1)} %slice.22), channel_id=1, source_target_pairs={{0,4},{4,8},{8,12},{1,5},{5,9},{9,13},{2,6},{6,10},{10,14},{3,7},{... | collective-permute-start | bytes 36872
  111.5 5.6 %collective-permute-start.4 = (bf16[12,512]{1,0:T(8,128)(2,1)S(1)}, bf16[12,512]{1,0:T(8,128)(2,1)S(1)}, u32[]{:S(2)}, u32[]{:S(2)}) collective-permute-start(bf16[12,512]{1,0:T(8,128)(2,1)S(1)} %slice.24), channel_id=1, source_target_pairs={{0,4},{4,8},{8,12},{1,5},{5,9},{9,13},{2,6},{6,10},{10,14},{3,7},{... | collective-permute-start | bytes 36872
  114.8 2.8 %collective-permute-start.1 = (bf16[12,512]{1,0:T(8,128)(2,1)S(1)}, bf16[12,512]{1,0:T(8,128)(2,1)S(1)}, u32[]{:S(2)}, u32[]{:S(2)}) collective-permute-start(bf16[12,512]{1,0:T(8,128)(2,1)S(1)} %slice.21), channel_id=1, source_target_pairs={{0,4},{4,8},{8,12},{1,5},{5,9},{9,13},{2,6},{6,10},{10,14},{3,7},{... | collective-permute-start | bytes 36872
  148.8 5.2 %collective-permute-start.5 = (bf16[12,1024]{1,0:T(8,128)(2,1)S(1)}, bf16[12,1024]{1,0:T(8,128)(2,1)S(1)}, u32[]{:S(2)}, u32[]{:S(2)}) collective-permute-start(bf16[12,1024]{1,0:T(8,128)(2,1)S(1)} %slice.25), channel_id=1, source_target_pairs={{0,1},{1,2},{2,3},{4,5},{5,6},{6,7},{8,9},{9,10},{10,11},{12,13},{... | collective-permute-start | bytes 73736
  220.5 7.8 %collective-permute-start.6 = (bf16[12,1024]{1,0:T(8,128)(2,1)S(1)}, bf16[12,1024]{1,0:T(8,128)(2,1)S(1)}, u32[]{:S(2)}, u32[]{:S(2)}) collective-permute-start(bf16[12,1024]{1,0:T(8,128)(2,1)S(1)} %slice.26), channel_id=1, source_target_pairs={{0,1},{1,2},{2,3},{4,5},{5,6},{6,7},{8,9},{9,10},{10,11},{12,13},{... | collective-permute-start | bytes 73736
Sparse Core Ops, SparseCore 0:
  21.9 39.3 all-reduce.22
  170.9 37.9 all-reduce.20
where the time goes:
time: 237 us; the launch traced here: 236 us
  blocking collectives  96.5 us (41%)
  waiting for transfers between devices  59 us (25%)
  matrix products  34.3 us (14%)
  starting transfers between devices  21.4 us (9%)
  between operations  16.5 us (7%)
  other arithmetic  5.63 us (2%)
  local copies, waits for them, and re-layouts  2.53 us (1%)
    psum x2, waiting for transfers between devices, feed_forward(): lax.psum(up_part.astype(jnp.bfloat16), 'kv').astype(jnp.float32)  57.7 us
    unnamed x5, blocking collectives  49.5 us
    unnamed x7, starting transfers between devices  21.3 us
    psum x2, blocking collectives, feed_forward(): lax.psum(squares.astype(jnp.bfloat16), 'kv').astype(jnp.float32)  19.4 us
    all_gather x3, blocking collectives, widen_rows(): return lax.all_gather(stream_rows, 'tp', axis=0, tiled=True)  17.3 us
    dot_general x2, matrix products, feed_forward(): up_part = jnp.dot(scaled, w_up, preferred_element_type=jnp.float32)  10.4 us
    all_gather x1, blocking collectives, retention(): return (lax.all_gather(ret_out, 'kv', axis=0, tiled=True), new_state)  10.3 us
    dot_general x3, matrix products, advance(): jnp.dot(inputs_back, weight_back, preferred_element_type=jnp.float32)  8.18 us
  transfers between devices with their start and end apart: 9, of which 4 were waited for; matrix products, arithmetic and copies ran while one was open for 2% of the time, Pallas kernels for 0%

commit v1 on v0

--- a/solution.py
+++ b/solution.py
@@ -6,6 +6,10 @@
 D = 4096
 EPS_NORM = 1e-06
 EPS_GROUP = 1e-05
+
+
+def pack_pools(field_in):
+    return jnp.sum(jax.lax.all_gather(field_in, "kv"), axis=0)
 
 
 def widen_rows(stream_rows):
@@ -25,7 +29,7 @@
     up_part = jnp.dot(scaled, w_up, preferred_element_type=jnp.float32)
     gate_part, up_part, squares = (
         lax.psum(gate_part.astype(jnp.bfloat16), "kv").astype(jnp.float32),
-        lax.psum(up_part.astype(jnp.bfloat16), "kv").astype(jnp.float32),
+        pack_pools(up_part.astype(jnp.bfloat16)).astype(jnp.float32),
         lax.psum(squares.astype(jnp.bfloat16), "kv").astype(jnp.float32),
     )
     factor = lax.rsqrt(squares / D + EPS_NORM)[:, None]

time: 237 us -> 284 us (1.20)
  waiting for transfers between devices: 59 us -> 97.1 us
  blocking collectives: 96.5 us -> 99.6 us
  matrix products: 34.3 us -> 37.3 us
  other arithmetic: 5.63 us -> 8.48 us
    all_gather x0 -> x2, waiting for transfers between devices: none -> 26.7 us  [pack_pools(): return jnp.sum(jax.lax.all_gather(field_in, 'kv'), axis=0)]
    psum x2, waiting for transfers between devices: 57.7 us -> 69.1 us  [feed_forward(): lax.psum(gate_part.astype(jnp.bfloat16), 'kv').astype(jnp.float32)]
    reduce_sum x0 -> x2, other arithmetic: none -> 2.84 us  [pack_pools(): return jnp.sum(jax.lax.all_gather(field_in, 'kv'), axis=0)]
  transfers between devices with their start and end apart: 9 -> 11, of which waited for: 4 -> 6; matrix products, arithmetic and copies ran while one was open for 2% -> 7% of each run, Pallas kernels for 0% -> 0%
where the time goes in v1:
time: 284 us; the launch traced here: 283 us
  blocking collectives  99.6 us (35%)
  waiting for transfers between devices  97.1 us (34%)
  matrix products  37.3 us (13%)
  starting transfers between devices  21.5 us (8%)
  between operations  16.2 us (6%)
  other arithmetic  8.48 us (3%)
    psum x2, waiting for transfers between devices, feed_forward(): lax.psum(gate_part.astype(jnp.bfloat16), 'kv').astype(jnp.float32)  69.1 us
    unnamed x5, blocking collectives  51.9 us
    all_gather x2, waiting for transfers between devices, pack_pools(): return jnp.sum(jax.lax.all_gather(field_in, 'kv'), axis=0)  26.7 us
    unnamed x7, starting transfers between devices  21.4 us
    psum x2, blocking collectives, feed_forward(): lax.psum(squares.astype(jnp.bfloat16), 'kv').astype(jnp.float32)  20.1 us
    all_gather x3, blocking collectives, widen_rows(): return lax.all_gather(stream_rows, 'tp', axis=0, tiled=True)  17.4 us
    all_gather x1, blocking collectives, retention(): return (lax.all_gather(ret_out, 'kv', axis=0, tiled=True), new_state)  10.2 us
    dot_general x2, matrix products, feed_forward(): up_part = jnp.dot(scaled, w_up, preferred_element_type=jnp.float32)  10.2 us
  transfers between devices with their start and end apart: 11, of which 6 were waited for; matrix products, arithmetic and copies ran while one was open for 7% of the time, Pallas kernels for 0%

profile of v1, /device:TPU:1, one launch (start us, length us, event | category | flops | bytes accessed | tf_op | source)
XLA Modules:
  0.0 282.8 jit_solution(12755864512717409412)
XLA Ops:
  7.2 6.7 %all-gather.2 = bf16[4,12,1024]{2,1,0:T(8,128)(2,1)S(1)} all-gather(bf16[1,12,1024]{2,1,0:T(8,128)(2,1)} %bitcast.47), channel_id=1, replica_groups=mesh['grp'=2,'kv'=4,'tp'=4] {'tp'}, dimensions={0}, use_global_device_ids=true | all-gather | bytes 122880 | tf_op jit(solution)/shard_map/all_gather | solution.py:16
  14.0 5.1 %convolution_convert_fusion.2 = bf16[48,2752]{1,0:T(8,128)(2,1)} fusion(bf16[1024,2752]{0,1:T(8,128)(2,1)} %param.23, bf16[48,1024]{1,0:T(8,128)(2,1)S(1)} %reshape.134, f32[1024]{0:T(1024)} %param.21), kind=kOutput, calls=%fused_computation.3 | convolution fusion | flops 270812160 | bytes 6002688 | tf_op jit(solution)/shard_map/dot_general | solution.py:29
  19.2 5.1 %convolution_convert_fusion.3 = bf16[48,2752]{1,0:T(8,128)(2,1)} fusion(bf16[1024,2752]{0,1:T(8,128)(2,1)} %param.22, bf16[48,1024]{1,0:T(8,128)(2,1)S(1)} %reshape.134, f32[1024]{0:T(1024)S(1)} %copy-done.4), kind=kOutput, calls=%fused_computation.4 | convolution fusion | flops 270812160 | bytes 6002688 | tf_op jit(solution)/shard_map/dot_general | solution.py:28
  24.5 11.0 %psum.28 = bf16[48]{0:T(256)(128)(2,1)S(1)} all-reduce(bf16[48]{0:T(256)(128)(2,1)S(1)} %fusion.14), channel_id=1, replica_groups=mesh['grp'=2,'kv'=4,'tp'=4] {'kv'}, use_global_device_ids=true, to_apply=%region_1.0 | all-reduce | flops 48 | bytes 192 | tf_op jit(solution)/shard_map/psum | solution.py:33
  35.7 12.9 %all-gather.9.cloned.1.call-done = bf16[192,2752]{1,0:T(8,128)(2,1)} async-done(((bf16[48,2752]{1,0:T(8,128)(2,1)}), bf16[192,2752]{1,0:T(8,128)(2,1)}) %all-gather.9.cloned.1.call-update) | async-done | bytes 1056784 | tf_op jit(solution)/shard_map/all_gather | solution.py:12
  48.6 1.4 reduce_sum.79
  50.0 34.7 %all-reduce.19.cloned.1.call-done = bf16[48,2752]{1,0:T(8,128)(2,1)} async-done(((bf16[48,2752]{1,0:T(8,128)(2,1)}), bf16[48,2752]{1,0:T(8,128)(2,1)}) %all-reduce.19.cloned.1.call-update) | async-done | bytes 264208 | tf_op jit(solution)/shard_map/psum | solution.py:31
  84.7 4.5 %convolution_convert_fusion.6 = bf16[48,1024]{1,0:T(8,128)(2,1)} fusion(bf16[2752,1024]{1,0:T(8,128)(2,1)} %param.24, bf16[48,2752]{1,0:T(8,128)(2,1)S(1)} %reduce_sum.79, bf16[48,2752]{1,0:T(8,128)(2,1)} %all-reduce.19.cloned.1.call-done, f32[48]{0:T(128)S(1)} %add_rsqrt_fusion.2), kind=kOutput, calls=%fused_computation.8 | convolution fusion | flops 271902720 | bytes 6262976 | tf_op jit(solution)/shard_map/dot_general | solution.py:42
  89.2 9.1 %fusion = bf16[16,1024]{1,0:T(8,128)(2,1)S(1)} fusion(bf16[48,1024]{1,0:T(8,128)(2,1)} %convolution_convert_fusion.6), kind=kCustom, calls=%all-reduce-scatter | all-reduce-scatter fusion | flops 65537 | bytes 131584
  98.3 4.2 %collective-permute-start = (bf16[12,1024]{1,0:T(8,128)(2,1)S(1)}, bf16[12,1024]{1,0:T(8,128)(2,1)S(1)}, u32[]{:S(2)}, u32[]{:S(2)}) collective-permute-start(bf16[12,1024]{1,0:T(8,128)(2,1)S(1)} %slice.20), channel_id=1, source_target_pairs={{0,1},{1,2},{2,3},{4,5},{5,6},{6,7},{8,9},{9,10},{10,11},{12,13},{... | collective-permute-start | bytes 73736
  102.5 0.6 dynamic-slice.18
  103.8 0.6 fusion.39
  105.7 0.2 concatenate.12
  105.9 4.4 %all-gather.3 = bf16[4,12,1024]{2,1,0:T(8,128)(2,1)S(1)} all-gather(bf16[1,12,1024]{2,1,0:T(8,128)(2,1)S(1)} %fusion.28), channel_id=1, replica_groups=mesh['grp'=2,'kv'=4,'tp'=4] {'tp'}, dimensions={0}, use_global_device_ids=true | all-gather | bytes 122880 | tf_op jit(solution)/shard_map/all_gather | solution.py:16
  110.4 9.0 %all-reduce.1 = bf16[48]{0:T(256)(128)(2,1)S(1)} all-reduce(bf16[48]{0:T(256)(128)(2,1)S(1)} %fusion.16), channel_id=5, replica_groups=mesh['grp'=2,'kv'=4,'tp'=4] {'kv'}, use_global_device_ids=true, to_apply=%region_6.7.clone | all-reduce | flops 48 | bytes 192
  119.4 0.3 convolution_convert_fusion.9
  119.7 0.3 convolution_convert_fusion.8
  120.0 1.5 convolution_convert_fusion.7
  121.5 1.5 convolution_convert_fusion.10
  123.0 10.4 %fusion.38 = (bf16[16,512]{1,0:T(8,128)(2,1)S(1)}, bf16[16,512]{1,0:T(8,128)(2,1)S(1)}, bf16[16,512]{1,0:T(8,128)(2,1)S(1)}, bf16[16,512]{1,0:T(8,128)(2,1)S(1)}) fusion(bf16[48,512]{1,0:T(8,128)(2,1)S(1)} %convolution_convert_fusion.10, bf16[48,512]{1,0:T(8,128)(2,1)S(1)} %convolution_convert_fusion.7, bf16[48,512]{1,0:T(8,128)(2,1)S(1)} %convolution_convert_fusion.9, ...), kind=kCustom, calls=%all-reduce-scatter.7 | all-reduce-scatter fusion | flops 131073 | bytes 262656
  133.6 1.7 collective-permute-start.3
  135.2 1.9 collective-permute-start.2
  137.2 3.3 %collective-permute-start.4 = (bf16[12,512]{1,0:T(8,128)(2,1)S(1)}, bf16[12,512]{1,0:T(8,128)(2,1)S(1)}, u32[]{:S(2)}, u32[]{:S(2)}) collective-permute-start(bf16[12,512]{1,0:T(8,128)(2,1)S(1)} %slice.24), channel_id=1, source_target_pairs={{0,4},{4,8},{8,12},{1,5},{5,9},{9,13},{2,6},{6,10},{10,14},{3,7},{... | collective-permute-start | bytes 36872
  140.4 1.9 collective-permute-start.1
  142.6 0.2 concatenate.14
  142.8 0.2 concatenate.16
  143.0 0.3 collective-permute-done.1
  143.7 4.6 %fusion.41 = f32[12,4,1,128]{3,2,1,0:T(1,128)S(1)} fusion(f32[12,4,128,1]{2,3,1,0:T(1,128)S(1)} %bitcast.46, f32[12,4,128,128]{3,2,1,0:T(8,128)} %param.20), kind=kOutput, calls=%fused_computation.70 | convolution fusion | flops 9437184 | bytes 3194880 | tf_op jit(solution)/shard_map/shd,shde->she/dot_general | solution.py:107
  148.3 0.2 fusion.40
  148.5 0.2 multiply_reduce_fusion
  148.8 10.2 %all-gather.4 = bf16[4,12,512]{2,1,0:T(8,128)(2,1)S(1)} all-gather(bf16[1,12,512]{2,1,0:T(8,128)(2,1)S(1)} %reshape.137), channel_id=1, replica_groups=mesh['grp'=2,'kv'=4,'tp'=4] {'kv'}, dimensions={0}, use_global_device_ids=true | all-gather | bytes 61440 | tf_op jit(solution)/shard_map/all_gather | solution.py:122
  159.1 0.3 convolution_convert_fusion.5
  159.4 15.0 %fusion.5 = bf16[16,1024]{1,0:T(8,128)(2,1)S(1)} fusion(bf16[48,1024]{1,0:T(8,128)(2,1)S(1)} %convolution_convert_fusion.5), kind=kCustom, calls=%all-reduce-scatter.5 | all-reduce-scatter fusion | flops 65537 | bytes 131584
  174.5 4.2 %collective-permute-start.5 = (bf16[12,1024]{1,0:T(8,128)(2,1)S(1)}, bf16[12,1024]{1,0:T(8,128)(2,1)S(1)}, u32[]{:S(2)}, u32[]{:S(2)}) collective-permute-start(bf16[12,1024]{1,0:T(8,128)(2,1)S(1)} %slice.25), channel_id=1, source_target_pairs={{0,1},{1,2},{2,3},{4,5},{5,6},{6,7},{8,9},{9,10},{10,11},{12,13},{... | collective-permute-start | bytes 73736
  178.7 1.0 collective-permute-done.5
  179.8 6.3 %all-gather.5 = bf16[4,12,1024]{2,1,0:T(8,128)(2,1)S(1)} all-gather(bf16[1,12,1024]{2,1,0:T(8,128)(2,1)S(1)} %fusion.29), channel_id=1, replica_groups=mesh['grp'=2,'kv'=4,'tp'=4] {'tp'}, dimensions={0}, use_global_device_ids=true | all-gather | bytes 122880 | tf_op jit(solution)/shard_map/all_gather | solution.py:16
  186.2 5.1 %convolution_convert_fusion = bf16[48,2752]{1,0:T(8,128)(2,1)} fusion(bf16[1024,2752]{0,1:T(8,128)(2,1)} %param.34, bf16[48,1024]{1,0:T(8,128)(2,1)S(1)} %reshape.140, f32[1024]{0:T(1024)S(1)} %copy-done.5), kind=kOutput, calls=%fused_computation.1 | convolution fusion | flops 270812160 | bytes 6002688 | tf_op jit(solution)/shard_map/dot_general | solution.py:29
  191.3 5.1 %convolution_convert_fusion.1 = bf16[48,2752]{1,0:T(8,128)(2,1)} fusion(bf16[1024,2752]{0,1:T(8,128)(2,1)} %param.33, bf16[48,1024]{1,0:T(8,128)(2,1)S(1)} %reshape.140, f32[1024]{0:T(1024)S(1)} %copy-done.5), kind=kOutput, calls=%fused_computation.2 | convolution fusion | flops 270812160 | bytes 6002688 | tf_op jit(solution)/shard_map/dot_general | solution.py:28
  196.6 9.1 %psum.30 = bf16[48]{0:T(256)(128)(2,1)S(1)} all-reduce(bf16[48]{0:T(256)(128)(2,1)S(1)} %fusion.18), channel_id=1, replica_groups=mesh['grp'=2,'kv'=4,'tp'=4] {'kv'}, use_global_device_ids=true, to_apply=%region_16.17 | all-reduce | flops 48 | bytes 192 | tf_op jit(solution)/shard_map/psum | solution.py:33
  205.7 13.8 %all-gather.11.cloned.1.call-done = bf16[192,2752]{1,0:T(8,128)(2,1)} async-done(((bf16[48,2752]{1,0:T(8,128)(2,1)}), bf16[192,2752]{1,0:T(8,128)(2,1)}) %all-gather.11.cloned.1.call-update) | async-done | bytes 1056784 | tf_op jit(solution)/shard_map/all_gather | solution.py:12
  219.5 1.4 reduce_sum.85
  220.9 34.4 %all-reduce.21.cloned.1.call-done = bf16[48,2752]{1,0:T(8,128)(2,1)} async-done(((bf16[48,2752]{1,0:T(8,128)(2,1)}), bf16[48,2752]{1,0:T(8,128)(2,1)}) %all-reduce.21.cloned.1.call-update) | async-done | bytes 264208 | tf_op jit(solution)/shard_map/psum | solution.py:31
  255.3 3.9 %convolution_convert_fusion.4 = bf16[48,1024]{1,0:T(8,128)(2,1)S(1)} fusion(bf16[2752,1024]{1,0:T(8,128)(2,1)} %param.35, bf16[48,2752]{1,0:T(8,128)(2,1)S(1)} %reduce_sum.85, bf16[48,2752]{1,0:T(8,128)(2,1)} %all-reduce.21.cloned.1.call-done, f32[48]{0:T(128)S(1)} %add_rsqrt_fusion.1), kind=kOutput, calls=%fused_computation.6 | convolution fusion | flops 271902720 | bytes 6262976 | tf_op jit(solution)/shard_map/dot_general | solution.py:42
  259.2 8.5 %fusion.6 = bf16[16,1024]{1,0:T(8,128)(2,1)S(1)} fusion(bf16[48,1024]{1,0:T(8,128)(2,1)S(1)} %convolution_convert_fusion.4), kind=kCustom, calls=%all-reduce-scatter.6 | all-reduce-scatter fusion | flops 65537 | bytes 131584
  267.6 4.2 %collective-permute-start.6 = (bf16[12,1024]{1,0:T(8,128)(2,1)S(1)}, bf16[12,1024]{1,0:T(8,128)(2,1)S(1)}, u32[]{:S(2)}, u32[]{:S(2)}) collective-permute-start(bf16[12,1024]{1,0:T(8,128)(2,1)S(1)} %slice.26), channel_id=1, source_target_pairs={{0,1},{1,2},{2,3},{4,5},{5,6},{6,7},{8,9},{9,10},{10,11},{12,13},{... | collective-permute-start | bytes 73736
  271.8 3.6 %multiply_add_fusion = f32[12,4,128,128]{3,2,1,0:T(8,128)} fusion(f32[12,4,128,128]{3,2,1,0:T(8,128)} %param.20, f32[12,4,128]{2,1,0:T(4,128)S(1)} %reshape.129, f32[12,4,128]{2,1,0:T(4,128)S(1)} %get-tuple-element.27, f32[4]{0:T(128)S(1)} %log-plus-one_exponential_fusion), kind=kLoop, calls=%fused_computation.5 | loop fusion | flops 2359296 | bytes 6340624 | tf_op jit(solution)/shard_map/add | solution.py:111
  275.4 0.2 concatenate.18
  275.6 0.7 add_convert_fusion
  (70 shorter events, 2.0 us)
Async XLA Ops:
  7.2 151.9 %copy-start = (bf16[512,1024]{1,0:T(8,128)(2,1)S(1)}, bf16[512,1024]{1,0:T(8,128)(2,1)}, u32[]{:S(2)}) copy-start(bf16[512,1024]{1,0:T(8,128)(2,1)} %param.30) | copy-start | bytes 3145732
  7.2 12.0 %copy-start.4 = (f32[1024]{0:T(1024)S(1)}, f32[1024]{0:T(1024)}, u32[]{:S(2)}) copy-start(f32[1024]{0:T(1024)} %param.21) | copy-start | bytes 12292
  7.2 41.4 %all-gather.9.cloned.1.call-start = ((), (), s32[]{:S(2)}) async-start(), calls=%async_computation.2 | async-start | bytes 1351680 | tf_op jit(solution)/shard_map/all_gather | solution.py:12
  14.0 21.6 %copy-start.9 = (s32[12]{0:T(128)S(1)}, s32[12]{0:T(128)}, u32[]{:S(2)}) copy-start(s32[12]{0:T(128)} %param.19) | copy-start | bytes 148
  19.1 65.6 %all-reduce.19.cloned.1.call-start = ((), (), s32[]{:S(2)}) async-start(), calls=%async_computation | async-start | bytes 540672 | tf_op jit(solution)/shard_map/psum | solution.py:31
  24.3 78.2 %copy-start.8 = (u32[32]{0:T(128)S(1)}, u32[32]{0:T(128)}, u32[]{:S(2)}) copy-start(u32[32]{0:T(128)} %constant.56) | copy-start | bytes 388
  24.3 79.5 %copy-start.7 = (u32[32]{0:T(128)S(1)}, u32[32]{0:T(128)}, u32[]{:S(2)}) copy-start(u32[32]{0:T(128)} %constant.60) | copy-start | bytes 388
  24.3 95.1 %copy-start.1 = (bf16[1024,512]{1,0:T(8,128)(2,1)S(1)}, bf16[1024,512]{1,0:T(8,128)(2,1)}, u32[]{:S(2)}) copy-start(bf16[1024,512]{1,0:T(8,128)(2,1)} %param.26) | copy-start | bytes 3145732
  24.3 95.1 %copy-start.3 = (f32[1024]{0:T(1024)S(1)}, f32[1024]{0:T(1024)}, u32[]{:S(2)}) copy-start(f32[1024]{0:T(1024)} %param.25) | copy-start | bytes 12292
  24.3 95.4 %copy-start.2 = (bf16[1024,512]{1,0:T(8,128)(2,1)S(1)}, bf16[1024,512]{1,0:T(8,128)(2,1)}, u32[]{:S(2)}) copy-start(bf16[1024,512]{1,0:T(8,128)(2,1)} %param.27) | copy-start | bytes 3145732
  24.3 195.2 %all-gather.11.cloned.1.call-start = ((), (), s32[]{:S(2)}) async-start(), calls=%async_computation.3 | async-start | bytes 1351680 | tf_op jit(solution)/shard_map/all_gather | solution.py:12
  89.2 59.5 %copy-start.6 = (f32[512]{0:T(512)S(1)}, f32[512]{0:T(512)}, u32[]{:S(2)}) copy-start(f32[512]{0:T(512)} %param.31) | copy-start | bytes 6148
  98.3 7.4 %collective-permute-start = (bf16[12,1024]{1,0:T(8,128)(2,1)S(1)}, bf16[12,1024]{1,0:T(8,128)(2,1)S(1)}, u32[]{:S(2)}, u32[]{:S(2)}) collective-permute-start(bf16[12,1024]{1,0:T(8,128)(2,1)S(1)} %slice.20), channel_id=1, source_target_pairs={{0,1},{1,2},{2,3},{4,5},{5,6},{6,7},{8,9},{9,10},{10,11},{12,13},{... | collective-permute-start | bytes 73736
  119.7 66.5 %copy-start.5 = (f32[1024]{0:T(1024)S(1)}, f32[1024]{0:T(1024)}, u32[]{:S(2)}) copy-start(f32[1024]{0:T(1024)} %param.32) | copy-start | bytes 12292
  133.6 8.9 %collective-permute-start.3 = (bf16[12,512]{1,0:T(8,128)(2,1)S(1)}, bf16[12,512]{1,0:T(8,128)(2,1)S(1)}, u32[]{:S(2)}, u32[]{:S(2)}) collective-permute-start(bf16[12,512]{1,0:T(8,128)(2,1)S(1)} %slice.23), channel_id=1, source_target_pairs={{0,4},{4,8},{8,12},{1,5},{5,9},{9,13},{2,6},{6,10},{10,14},{3,7},{... | collective-permute-start | bytes 36872
  135.2 7.4 %collective-permute-start.2 = (bf16[12,512]{1,0:T(8,128)(2,1)S(1)}, bf16[12,512]{1,0:T(8,128)(2,1)S(1)}, u32[]{:S(2)}, u32[]{:S(2)}) collective-permute-start(bf16[12,512]{1,0:T(8,128)(2,1)S(1)} %slice.22), channel_id=1, source_target_pairs={{0,4},{4,8},{8,12},{1,5},{5,9},{9,13},{2,6},{6,10},{10,14},{3,7},{... | collective-permute-start | bytes 36872
  137.2 5.6 %collective-permute-start.4 = (bf16[12,512]{1,0:T(8,128)(2,1)S(1)}, bf16[12,512]{1,0:T(8,128)(2,1)S(1)}, u32[]{:S(2)}, u32[]{:S(2)}) collective-permute-start(bf16[12,512]{1,0:T(8,128)(2,1)S(1)} %slice.24), channel_id=1, source_target_pairs={{0,4},{4,8},{8,12},{1,5},{5,9},{9,13},{2,6},{6,10},{10,14},{3,7},{... | collective-permute-start | bytes 36872
  140.4 2.8 collective-permute-start.1
  174.5 5.2 %collective-permute-start.5 = (bf16[12,1024]{1,0:T(8,128)(2,1)S(1)}, bf16[12,1024]{1,0:T(8,128)(2,1)S(1)}, u32[]{:S(2)}, u32[]{:S(2)}) collective-permute-start(bf16[12,1024]{1,0:T(8,128)(2,1)S(1)} %slice.25), channel_id=1, source_target_pairs={{0,1},{1,2},{2,3},{4,5},{5,6},{6,7},{8,9},{9,10},{10,11},{12,13},{... | collective-permute-start | bytes 73736
  191.3 64.0 %all-reduce.21.cloned.1.call-start = ((), (), s32[]{:S(2)}) async-start(), calls=%async_computation.1 | async-start | bytes 540672 | tf_op jit(solution)/shard_map/psum | solution.py:31
  267.6 7.8 %collective-permute-start.6 = (bf16[12,1024]{1,0:T(8,128)(2,1)S(1)}, bf16[12,1024]{1,0:T(8,128)(2,1)S(1)}, u32[]{:S(2)}, u32[]{:S(2)}) collective-permute-start(bf16[12,1024]{1,0:T(8,128)(2,1)S(1)} %slice.26), channel_id=1, source_target_pairs={{0,1},{1,2},{2,3},{4,5},{5,6},{6,7},{8,9},{9,10},{10,11},{12,13},{... | collective-permute-start | bytes 73736
Sparse Core Ops, SparseCore 0:
  19.2 29.2 all-gather.8
  50.9 33.7 all-reduce.18
  191.4 28.0 all-gather.10
  221.7 33.5 all-reduce.20
